TPU v7x, 32 devices: a whole 2x2x4 slice. The times are simulated.
32 devices in a mesh: sp: 4 (over y, x), tp: 8 (over z, core).
Axes of the slice: x: 2, y: 2, z: 4, core: 2. Of those that a mesh axis runs over, the one named last changes fastest.
Arguments:
- query_a: bfloat16 [512, 16, 256], P('sp', 'tp'), may hold values from -5.5 to 5.5
- key_a: bfloat16 [512, 16, 256], P('sp', 'tp'), may hold values from -5.5 to 5.5
- value_a: bfloat16 [512, 16, 256], P('sp', 'tp'), may hold values from -6 to 6
- query_b: bfloat16 [512, 16, 128], P('sp', 'tp'), may hold values from -5.5 to 5.5
- key_b: bfloat16 [512, 16, 128], P('sp', 'tp'), may hold values from -5.5 to 5.5
- value_b: bfloat16 [512, 16, 128], P('sp', 'tp'), may hold values from -6 to 6
- lambdas: float32 [2, 16], P(None, 'tp'), may hold values from 0.3 to 0.8
- gain_a: float32 [256], replicated, may hold values from 0.1 to 1.9
- gain_b: float32 [128], replicated, may hold values from 0.1 to 1.9
- out_a: bfloat16 [4096, 4096], P('tp'), may hold values from -0.078125 to 0.078125
- out_b: bfloat16 [2048, 4096], P('tp'), may hold values from -0.078125 to 0.078125
- residual: bfloat16 [512, 4096], P(('sp', 'tp')), may hold values from -6 to 6
- norm_gain: float32 [4096], replicated, may hold values from 0.1 to 1.9
- route_ids: int32 [512, 2], P(('sp', 'tp')), may hold values from 0 to 7, all different within a row; in each aligned block of 16 rows (0 to 15, 16 to 31, ...) at most 8 rows name the same one
- route_weights: float32 [512, 2], P(('sp', 'tp')), may hold values from 0.1 to 0.9
- w_gate: bfloat16 [8, 4096, 2048], P('sp', None, 'tp'), may hold values from -0.28125 to 0.28125
- w_up: bfloat16 [8, 4096, 2048], P('sp', None, 'tp'), may hold values from -0.28125 to 0.28125
- w_down: bfloat16 [8, 2048, 4096], P('sp', 'tp'), may hold values from -0.01977539 to 0.01977539
Outputs:
- result: bfloat16 [512, 4096], P(('sp', 'tp'))
Inputs may be any that keep to these rules, and one draw needn't show every extreme that they name: `route_ids`: in the rows of one device each token names 2 different experts, no expert is named more than 8 times, a bound that some block reaches.
All inputs are finite; a program needn't handle non-finite values.
Results may differ from a plain program's by a relative error of at most 0.02.
Values may be sent and summed in bfloat16 or wider, within the bound.
A program may use at most 128 MiB of HBM per device.

v0:
```python
import jax
import jax.numpy as jnp
from jax import lax
from jax.sharding import PartitionSpec as P

EPSILON = 1e-06
LIMIT = 7.0
SLOPE = 1.702
FLOOR = -1e30


def empty_state(heads_here, queries_here, value_width):
    maxima = jnp.full((2, heads_here, queries_here), FLOOR, jnp.float32)
    totals = jnp.zeros((2, heads_here, queries_here), jnp.float32)
    sums = jnp.zeros((2, heads_here, queries_here, value_width), jnp.float32)
    return (maxima, totals, sums)


def absorb_keys(states, queries, keys, values, width):
    maxima, totals, sums = states
    scaling = width ** (-0.5)
    new_maxima = []
    new_totals = []
    new_sums = []
    for which in range(2):
        query_part = queries[:, :, which * width : (which + 1) * width]
        key_part = keys[:, :, which * width : (which + 1) * width]
        scores = (
            jnp.einsum("qhd,khd->hqk", query_part, key_part, preferred_element_type=jnp.float32)
            * scaling
        )
        highest = jnp.maximum(maxima[which], jnp.max(scores, axis=2))
        expo = jnp.exp(scores - highest[:, :, None])
        factor = jnp.exp(maxima[which] - highest)
        new_totals.append(totals[which] * factor + jnp.sum(expo, axis=2))
        carried = jnp.einsum(
            "hqk,khv->hqv", expo.astype(jnp.bfloat16), values, preferred_element_type=jnp.float32
        )
        new_sums.append(sums[which] * factor[:, :, None] + carried)
        new_maxima.append(highest)
    return (jnp.stack(new_maxima), jnp.stack(new_totals), jnp.stack(new_sums))


def finish(states, lambda_row, gain):
    maxima, totals, sums = states
    heard = sums / totals[:, :, :, None]
    differ = heard[0] - lambda_row[:, None, None] * heard[1]
    scaled = lax.rsqrt(jnp.mean(differ * differ, axis=2, keepdims=True) + EPSILON)
    return (differ * scaled * gain).astype(jnp.bfloat16)


def gated_units(grid, w_gate, w_up):
    gate = jnp.einsum("necd,edf->necf", grid, w_gate, preferred_element_type=jnp.float32)
    upward = jnp.einsum("necd,edf->necf", grid, w_up, preferred_element_type=jnp.float32)
    clamped = jnp.minimum(gate, LIMIT)
    return (
        clamped * jax.nn.sigmoid(SLOPE * clamped) * (jnp.clip(upward, -LIMIT, LIMIT) + 1.0)
    ).astype(jnp.bfloat16)


def per_device(
    query_a,
    key_a,
    value_a,
    query_b,
    key_b,
    value_b,
    lambdas,
    gain_a,
    gain_b,
    out_a,
    out_b,
    residual,
    norm_gain,
    route_ids,
    route_weights,
    w_gate,
    w_up,
    w_down,
):
    heads_here = query_a.shape[1]
    queries_here = query_a.shape[0]
    width_a = query_a.shape[2] // 2
    width_b = query_b.shape[2] // 2
    starting = (
        empty_state(heads_here, queries_here, value_a.shape[2]),
        empty_state(heads_here, queries_here, value_b.shape[2]),
    )
    keys_a = lax.all_gather(key_a, "sp", axis=0, tiled=True)
    values_a = lax.all_gather(value_a, "sp", axis=0, tiled=True)
    keys_b = lax.all_gather(key_b, "sp", axis=0, tiled=True)
    values_b = lax.all_gather(value_b, "sp", axis=0, tiled=True)
    state_a = absorb_keys(starting[0], query_a, keys_a, values_a, width_a)
    state_b = absorb_keys(starting[1], query_b, keys_b, values_b, width_b)
    attended_a = finish(state_a, lambdas[0], gain_a)
    attended_b = finish(state_b, lambdas[1], gain_b)
    model_width = out_a.shape[1]
    weights_a = out_a.reshape(heads_here, -1, model_width)
    weights_b = out_b.reshape(heads_here, -1, model_width)
    first = jnp.einsum("hqv,hvd->qd", attended_a, weights_a, preferred_element_type=jnp.float32)
    projected = lax.psum_scatter(
        (
            first
            + jnp.einsum("hqv,hvd->qd", attended_b, weights_b, preferred_element_type=jnp.float32)
        ).astype(jnp.bfloat16),
        "tp",
        scatter_dimension=0,
        tiled=True,
    ).astype(jnp.float32)
    mixed = (residual.astype(jnp.float32) + projected).astype(jnp.bfloat16)
    widened = mixed.astype(jnp.float32)
    normed = (
        widened
        * lax.rsqrt(jnp.mean(widened * widened, axis=1, keepdims=True) + EPSILON)
        * norm_gain
    ).astype(jnp.bfloat16)
    rows_here, chosen = route_ids.shape
    groups = lax.axis_size("sp")
    experts_here = w_gate.shape[0]
    experts_all = experts_here * groups
    capacity = 2 * rows_here * chosen // experts_all
    slots_here = experts_here * capacity
    flat_ids = route_ids.reshape(-1)
    onehot = (flat_ids[:, None] == jnp.arange(experts_all, dtype=jnp.int32)[None, :]).astype(
        jnp.int32
    )
    earlier = jnp.cumsum(onehot, axis=0) - onehot
    target = flat_ids * capacity + jnp.sum(earlier * onehot, axis=1)
    places = jnp.arange(experts_all * capacity, dtype=jnp.int32)
    layout = jnp.any(target.reshape(rows_here, chosen)[None, :, :] == places[:, None, None], axis=2)
    outgoing = jnp.dot(
        layout.astype(jnp.bfloat16), normed, preferred_element_type=jnp.float32
    ).astype(jnp.bfloat16)
    outgoing = outgoing.reshape(groups, slots_here, model_width)
    arrived = lax.all_to_all(outgoing, "sp", split_axis=0, concat_axis=0, tiled=True)
    pieces = lax.all_gather(arrived, "tp", axis=0, tiled=True)
    count = pieces.shape[0]
    grid = pieces.reshape(count, experts_here, capacity, model_width)
    active = gated_units(grid, w_gate, w_up)
    down = jnp.einsum("necf,efd->necd", active, w_down, preferred_element_type=jnp.float32)
    partial_value = down.astype(jnp.bfloat16).reshape(count, slots_here, model_width)
    totals = lax.psum_scatter(
        partial_value.astype(jnp.float32).astype(jnp.bfloat16),
        "tp",
        scatter_dimension=0,
        tiled=True,
    )
    summed = lax.all_to_all(totals, "sp", split_axis=0, concat_axis=0, tiled=True)
    results = summed.reshape(experts_all * capacity, model_width)
    picked = (
        jnp.take(results, target, axis=0)
        .reshape(rows_here, chosen, model_width)
        .astype(jnp.float32)
    )
    combined = jnp.sum(route_weights[:, :, None] * picked, axis=1)
    return (widened + combined).astype(jnp.bfloat16)


def solution(mesh):
    in_specs = (
        P("sp", "tp", None),
        P("sp", "tp", None),
        P("sp", "tp", None),
        P("sp", "tp", None),
        P("sp", "tp", None),
        P("sp", "tp", None),
        P(None, "tp"),
        P(),
        P(),
        P("tp", None),
        P("tp", None),
        P(("sp", "tp"), None),
        P(),
        P(("sp", "tp"), None),
        P(("sp", "tp"), None),
        P("sp", None, "tp"),
        P("sp", None, "tp"),
        P("sp", "tp", None),
    )
    out_specs = P(("sp", "tp"), None)
    return jax.shard_map(
        per_device, mesh=mesh, in_specs=in_specs, out_specs=out_specs, check_vma=False
    )
```

profile of v0, /device:TPU:0, one launch (start us, length us, event | category | flops | bytes accessed | tf_op | source)
XLA Modules:
  0.0 234.9 jit_solution(8185951982461286773)
XLA Ops:
  6.5 1.1 copy.77
  7.6 11.5 %all_gather.15 = bf16[512,2,256]{2,0,1:T(8,128)(2,1)S(1)} all-gather(bf16[128,2,256]{2,0,1:T(8,128)(2,1)S(1)} %copy.77), channel_id=1, replica_groups=mesh['sp'=4,'tp'=8] {'sp'}, dimensions={0}, use_global_device_ids=true | all-gather | bytes 655360 | tf_op jit(solution)/shard_map/all_gather | solution.py:89
  19.1 1.0 fusion.120
  20.2 0.3 fusion.125
  20.5 0.3 fusion.124
  20.8 1.0 copy.78
  21.8 10.2 %all_gather.16 = bf16[512,2,256]{2,0,1:T(8,128)(2,1)S(1)} all-gather(bf16[128,2,256]{2,0,1:T(8,128)(2,1)S(1)} %copy.78), channel_id=1, replica_groups=mesh['sp'=4,'tp'=8] {'sp'}, dimensions={0}, use_global_device_ids=true | all-gather | bytes 655360 | tf_op jit(solution)/shard_map/all_gather | solution.py:90
  32.4 0.3 fusion.50
  32.7 0.3 fusion.49
  33.2 0.8 copy-done.2
  34.3 8.6 %all_gather.17 = bf16[512,2,128]{0,2,1:T(8,128)(2,1)S(1)} all-gather(bf16[128,2,128]{0,2,1:T(8,128)(2,1)S(1)} %copy.81), channel_id=1, replica_groups=mesh['sp'=4,'tp'=8] {'sp'}, dimensions={0}, use_global_device_ids=true | all-gather | bytes 327680 | tf_op jit(solution)/shard_map/all_gather | solution.py:91
  43.0 0.3 fusion.123
  43.3 0.3 fusion.122
  43.8 9.0 %all_gather.18 = bf16[512,2,128]{0,2,1:T(8,128)(2,1)S(1)} all-gather(bf16[128,2,128]{0,2,1:T(8,128)(2,1)S(1)} %copy.82), channel_id=1, replica_groups=mesh['sp'=4,'tp'=8] {'sp'}, dimensions={0}, use_global_device_ids=true | all-gather | bytes 327680 | tf_op jit(solution)/shard_map/all_gather | solution.py:92
  53.3 0.3 fusion.52
  53.6 0.3 fusion.51
  54.1 0.6 convolution_bitcast_fusion
  54.7 1.8 fusion.2
  57.4 32.2 %reduce-scatter.3.cloned.1.call-done = bf16[16,4096]{1,0:T(8,128)(2,1)} async-done(((bf16[128,4096]{1,0:T(8,128)(2,1)}), bf16[16,4096]{1,0:T(8,128)(2,1)}) %reduce-scatter.3.cloned.1.call-update) | async-done | bytes 131088 | tf_op jit(solution)/shard_map/reduce_scatter | solution.py:101
  89.6 1.1 fusion.67
  90.7 1.2 convolution_convert_fusion.1
  91.9 11.0 %all_to_all.10 = bf16[4,16,4096]{2,1,0:T(8,128)(2,1)} all-to-all(bf16[4,16,4096]{2,1,0:T(8,128)(2,1)S(1)} %bitcast.129), channel_id=1, replica_groups=mesh['sp'=4,'tp'=8] {'sp'}, dimensions={0} | all-to-all | bytes 1048576 | tf_op jit(solution)/shard_map/all_to_all | solution.py:135
  103.0 45.4 %all-gather.2.cloned.1.call-done = bf16[32,16,4096]{2,1,0:T(8,128)(2,1)} async-done(((bf16[4,16,4096]{2,1,0:T(8,128)(2,1)}), bf16[32,16,4096]{2,1,0:T(8,128)(2,1)}) %all-gather.2.cloned.1.call-update) | async-done | bytes 4194320 | tf_op jit(solution)/shard_map/all_gather | solution.py:136
  148.3 4.7 %fusion.15 = f32[32,2,8,256]{3,2,0,1:T(8,128)S(1)} fusion(bf16[2,4096,256]{2,1,0:T(8,128)(2,1)} %param.33, bf16[32,16,4096]{2,1,0:T(8,128)(2,1)} %all-gather.2.cloned.1.call-done), kind=kOutput, calls=%fused_computation.21 | convolution fusion | flops 1073872896 | bytes 8912896 | tf_op jit(solution)/shard_map/necd,edf->necf/dot_general | solution.py:53
  153.1 9.1 %fusion = bf16[32,2,8,4096]{3,2,0,1:T(8,128)(2,1)} fusion(bf16[2,256,4096]{2,1,0:T(8,128)(2,1)} %param.35, bf16[2,4096,256]{2,1,0:T(8,128)(2,1)} %param.34, f32[32,2,8,256]{3,2,0,1:T(8,128)S(1)} %fusion.15, bf16[32,16,4096]{2,1,0:T(8,128)(2,1)} %all-gather.2.cloned.1.call-done), kind=kOutput, calls=%fused_computation.2 | convolution fusion | flops 2150760448 | bytes 17301504 | tf_op jit(solution)/shard_map/necf,efd->necd/dot_general | solution.py:140
  162.2 4.6 %copy.138 = bf16[32,2,8,4096]{3,2,1,0:T(8,128)(2,1)} copy(bf16[32,2,8,4096]{3,2,0,1:T(8,128)(2,1)} %fusion) | data formatting | bytes 8388608 | tf_op jit(solution)/shard_map/convert_element_type | solution.py:141
  166.8 48.9 %reduce-scatter.5.cloned.1.call-done = bf16[4,16,4096]{2,1,0:T(8,128)(2,1)} async-done(((bf16[32,16,4096]{2,1,0:T(8,128)(2,1)}), bf16[4,16,4096]{2,1,0:T(8,128)(2,1)}) %reduce-scatter.5.cloned.1.call-update) | async-done | bytes 524304 | tf_op jit(solution)/shard_map/reduce_scatter | solution.py:142
  215.7 3.6 %all-to-all-start.1 = ((bf16[4,16,4096]{2,1,0:T(8,128)(2,1)}), bf16[4,16,4096]{2,1,0:T(8,128)(2,1)S(1)}, u32[]{:S(2)}, u32[]{:S(2)}) async-start(bf16[4,16,4096]{2,1,0:T(8,128)(2,1)} %reduce-scatter.5.cloned.1.call-done), calls=%async_computation.3 | async-start | bytes 1048576 | tf_op jit(solution)/shard_map/all_to_all | solution.py:148
  219.7 6.2 %all-to-all-done.1 = bf16[4,16,4096]{2,1,0:T(8,128)(2,1)S(1)} async-done(((bf16[4,16,4096]{2,1,0:T(8,128)(2,1)}), bf16[4,16,4096]{2,1,0:T(8,128)(2,1)S(1)}, u32[]{:S(2)}, u32[]{:S(2)}) %all-to-all-start.1) | async-done | bytes 524320 | tf_op jit(solution)/shard_map/all_to_all | solution.py:148
  225.9 0.7 gather_fusion
  226.8 0.8 multiply_reduce_fusion
  227.7 0.7 fusion.70
  (75 shorter events, 3.3 us)
Async XLA Ops:
  6.5 47.6 %copy-start = (bf16[256,4096]{1,0:T(8,128)(2,1)S(1)}, bf16[256,4096]{1,0:T(8,128)(2,1)}, u32[]{:S(2)}) copy-start(bf16[256,4096]{1,0:T(8,128)(2,1)} %param.28) | copy-start | bytes 6291460
  6.5 26.5 %copy-start.13 = (f32[2,2]{1,0:T(2,128)S(1)}, f32[2,2]{1,0:T(2,128)}, u32[]{:S(2)}) copy-start(f32[2,2]{1,0:T(2,128)} %param.24) | copy-start | bytes 52
  6.5 83.1 %reduce-scatter.3.cloned.1.call-start = ((), (), s32[]{:S(2)}) async-start(), calls=%async_computation.4 | async-start | bytes 1179648 | tf_op jit(solution)/shard_map/reduce_scatter | solution.py:101
  19.1 15.1 %copy-start.7 = (bf16[128,2,128]{2,1,0:T(2,128)(2,1)S(1)}, bf16[128,2,128]{2,1,0:T(2,128)(2,1)}, u32[]{:S(2)}) copy-start(bf16[128,2,128]{2,1,0:T(2,128)(2,1)} %param.22) | copy-start | bytes 196612
  20.1 22.8 %copy-start.6 = (bf16[128,2,128]{2,1,0:T(2,128)(2,1)S(1)}, bf16[128,2,128]{2,1,0:T(2,128)(2,1)}, u32[]{:S(2)}) copy-start(bf16[128,2,128]{2,1,0:T(2,128)(2,1)} %param.21) | copy-start | bytes 196612
  20.8 22.8 %copy-start.8 = (bf16[128,2,128]{2,1,0:T(2,128)(2,1)S(1)}, bf16[128,2,128]{2,1,0:T(2,128)(2,1)}, u32[]{:S(2)}) copy-start(bf16[128,2,128]{2,1,0:T(2,128)(2,1)} %param.23) | copy-start | bytes 196612
  33.0 21.1 %copy-start.14 = (f32[128]{0:T(128)S(1)}, f32[128]{0:T(128)}, u32[]{:S(2)}) copy-start(f32[128]{0:T(128)} %param.26) | copy-start | bytes 1540
  33.2 0.8 copy-start.2
  43.8 10.9 %copy-start.1 = (bf16[512,4096]{1,0:T(8,128)(2,1)S(1)}, bf16[512,4096]{1,0:T(8,128)(2,1)}, u32[]{:S(2)}) copy-start(bf16[512,4096]{1,0:T(8,128)(2,1)} %param.27) | copy-start | bytes 12582916
  43.8 10.9 %copy-start.3 = (f32[2,2,128,256]{3,2,1,0:T(8,128)S(1)}, f32[2,2,128,256]{3,2,1,0:T(8,128)}, u32[]{:S(2)}) copy-start(f32[2,2,128,256]{3,2,1,0:T(8,128)} %copy-done.2) | copy-start | bytes 1572868
  43.8 10.9 %copy-start.11 = (f32[256]{0:T(256)S(1)}, f32[256]{0:T(256)}, u32[]{:S(2)}) copy-start(f32[256]{0:T(256)} %param.25) | copy-start | bytes 3076
  54.7 1.9 copy-start.10
  54.7 34.9 %copy-start.4 = (bf16[16,4096]{1,0:T(8,128)(2,1)S(1)}, bf16[16,4096]{1,0:T(8,128)(2,1)}, u32[]{:S(2)}) copy-start(bf16[16,4096]{1,0:T(8,128)(2,1)} %param.29) | copy-start | bytes 393220
  54.7 35.9 %copy-start.9 = (f32[4096]{0:T(1024)S(1)}, f32[4096]{0:T(1024)}, u32[]{:S(2)}) copy-start(f32[4096]{0:T(1024)} %param.30) | copy-start | bytes 49156
  56.6 91.7 %all-gather.2.cloned.1.call-start = ((), (), s32[]{:S(2)}) async-start(), calls=%async_computation.5 | async-start | bytes 4718592 | tf_op jit(solution)/shard_map/all_gather | solution.py:136
  102.9 112.8 %reduce-scatter.5.cloned.1.call-start = ((), (), s32[]{:S(2)}) async-start(), calls=%async_computation.6 | async-start | bytes 4718592 | tf_op jit(solution)/shard_map/reduce_scatter | solution.py:142
  166.8 52.8 %copy-start.12 = (f32[16,2]{0,1:T(2,128)S(1)}, f32[16,2]{0,1:T(2,128)}, u32[]{:S(2)}) copy-start(f32[16,2]{0,1:T(2,128)} %param.32) | copy-start | bytes 388
  166.8 60.9 %copy-start.5 = (bf16[16,4096]{1,0:T(8,128)(2,1)S(1)}, bf16[16,4096]{1,0:T(8,128)(2,1)}, u32[]{:S(2)}) copy-start(bf16[16,4096]{1,0:T(8,128)(2,1)} %reduce-scatter.3.cloned.1.call-done) | copy-start | bytes 393220
  215.7 10.2 %all-to-all-start.1 = ((bf16[4,16,4096]{2,1,0:T(8,128)(2,1)}), bf16[4,16,4096]{2,1,0:T(8,128)(2,1)S(1)}, u32[]{:S(2)}, u32[]{:S(2)}) async-start(bf16[4,16,4096]{2,1,0:T(8,128)(2,1)} %reduce-scatter.5.cloned.1.call-done), calls=%async_computation.3 | async-start | bytes 1048576 | tf_op jit(solution)/shard_map/all_to_all | solution.py:148
Sparse Core Ops, SparseCore 0:
  56.7 32.8 reduce-scatter.2
  103.0 45.2 all-gather.1
  166.9 48.7 reduce-scatter.4
where the time goes:
time: 235 us
  waiting for transfers between devices  133 us (57%)
  blocking collectives  50.2 us (21%)
  matrix products  19.9 us (8%)
  between operations  13.5 us (6%)
  local copies, waits for them, and re-layouts  10.5 us (4%)
  other arithmetic  4.46 us (2%)
  starting transfers between devices  3.72 us (2%)
    reduce_scatter x1, waiting for transfers between devices, per_device(): lax.psum_scatter(partial_value.astype(jnp.float32).astype(jnp.bfloat16),...  48.9 us
    all_gather x1, waiting for transfers between devices, per_device(): pieces = lax.all_gather(arrived, 'tp', axis=0, tiled=True)  45.4 us
    reduce_scatter x1, waiting for transfers between devices, per_device(): lax.psum_scatter((first + jnp.einsum('hqv,hvd->qd', attended_b, weights_b...  32.2 us
    all_gather x1, blocking collectives, per_device(): keys_a = lax.all_gather(key_a, 'sp', axis=0, tiled=True)  11.5 us
    all_to_all x1, blocking collectives, per_device(): lax.all_to_all(outgoing, 'sp', split_axis=0, concat_axis=0, tiled=True)  11 us
    all_gather x1, blocking collectives, per_device(): values_a = lax.all_gather(value_a, 'sp', axis=0, tiled=True)  10.2 us
    dot_general x1, matrix products, per_device(): jnp.einsum('necf,efd->necd', active, w_down, preferred_element_type=jnp.f...  9.1 us
    all_gather x1, blocking collectives, per_device(): values_b = lax.all_gather(value_b, 'sp', axis=0, tiled=True)  9.03 us
  transfers between devices with their start and end apart: 4, of which 4 were waited for; matrix products, arithmetic and copies ran while one was open for 0% of the time, Pallas kernels for 0%

commit v1 on v0

--- a/solution.py
+++ b/solution.py
@@ -133,7 +133,12 @@
     ).astype(jnp.bfloat16)
     outgoing = outgoing.reshape(groups, slots_here, model_width)
     arrived = lax.all_to_all(outgoing, "sp", split_axis=0, concat_axis=0, tiled=True)
-    pieces = lax.all_gather(arrived, "tp", axis=0, tiled=True)
+    ring = [arrived]
+    for hop in range(7):
+        ring.append(lax.ppermute(ring[-1], "tp", [(dev, (dev + 1) % 8) for dev in range(8)]))
+    pieces = jnp.roll(
+        jnp.concatenate(ring[::-1], axis=0), (lax.axis_index("tp") + 1) * ring[0].shape[0], axis=0
+    )
     count = pieces.shape[0]
     grid = pieces.reshape(count, experts_here, capacity, model_width)
     active = gated_units(grid, w_gate, w_up)

time: 235 us -> 275 us (1.17)
  waiting for transfers between devices: 133 us -> 158 us
  local copies, waits for them, and re-layouts: 10.5 us -> 27.8 us
  matrix products: 19.9 us -> 16.3 us
    ppermute x0 -> x7, waiting for transfers between devices: none -> 73.2 us  [per_device(): lax.ppermute(ring[-1], 'tp', [(dev, (dev + 1) % 8) for dev in range(8)])]
    all_gather x1 -> x0, waiting for transfers between devices: 45.4 us -> none  [per_device(): pieces = lax.all_gather(arrived, 'tp', axis=0, tiled=True)]
    unnamed x36 -> x61, local copies, waits for them, and re-layouts: 3.29 us -> 18.6 us
    dot_general x1, matrix products: 4.71 us -> 1.25 us  [gated_units(): jnp.einsum('necd,edf->necf', grid, w_gate, preferred_element_type=jnp.flo...]
  transfers between devices with their start and end apart: 4 -> 10, of which waited for: 4 -> 10; matrix products, arithmetic and copies ran while one was open for 0% -> 0% of each run, Pallas kernels for 0% -> 0%
where the time goes in v1:
time: 275 us; the launch traced here: 274 us
  waiting for transfers between devices  158 us (57%)
  blocking collectives  49.3 us (18%)
  local copies, waits for them, and re-layouts  27.8 us (10%)
  matrix products  16.3 us (6%)
  between operations  13.9 us (5%)
  other arithmetic  4.43 us (2%)
  starting transfers between devices  3.71 us (1%)
    ppermute x7, waiting for transfers between devices, per_device(): lax.ppermute(ring[-1], 'tp', [(dev, (dev + 1) % 8) for dev in range(8)])  73.2 us
    reduce_scatter x1, waiting for transfers between devices, per_device(): lax.psum_scatter(partial_value.astype(jnp.float32).astype(jnp.bfloat16),...  46.8 us
    reduce_scatter x1, waiting for transfers between devices, per_device(): lax.psum_scatter((first + jnp.einsum('hqv,hvd->qd', attended_b, weights_b...  32.2 us
    unnamed x61, local copies, waits for them, and re-layouts  18.6 us
    all_to_all x1, blocking collectives, per_device(): lax.all_to_all(outgoing, 'sp', split_axis=0, concat_axis=0, tiled=True)  10.5 us
    all_gather x1, blocking collectives, per_device(): keys_b = lax.all_gather(key_b, 'sp', axis=0, tiled=True)  10.5 us
    all_gather x1, blocking collectives, per_device(): keys_a = lax.all_gather(key_a, 'sp', axis=0, tiled=True)  9.74 us
    all_gather x1, blocking collectives, per_device(): values_a = lax.all_gather(value_a, 'sp', axis=0, tiled=True)  9.66 us
  transfers between devices with their start and end apart: 10, of which 10 were waited for; matrix products, arithmetic and copies ran while one was open for 0% of the time, Pallas kernels for 0%

profile of v1, /device:TPU:0, one launch (start us, length us, event | category | flops | bytes accessed | tf_op | source)
XLA Modules:
  0.0 273.8 jit_solution(1752320583373839860)
XLA Ops:
  6.5 1.1 copy.66
  7.7 10.5 %all_gather.14 = bf16[512,2,128]{0,2,1:T(8,128)(2,1)S(1)} all-gather(bf16[128,2,128]{0,2,1:T(8,128)(2,1)S(1)} %copy.66), channel_id=1, replica_groups=mesh['sp'=4,'tp'=8] {'sp'}, dimensions={0}, use_global_device_ids=true | all-gather | bytes 327680 | tf_op jit(solution)/shard_map/all_gather | solution.py:91
  20.8 9.0 %all_gather.15 = bf16[512,2,128]{0,2,1:T(8,128)(2,1)S(1)} all-gather(bf16[128,2,128]{0,2,1:T(8,128)(2,1)S(1)} %copy.67), channel_id=1, replica_groups=mesh['sp'=4,'tp'=8] {'sp'}, dimensions={0}, use_global_device_ids=true | all-gather | bytes 327680 | tf_op jit(solution)/shard_map/all_gather | solution.py:92
  30.9 1.1 slice_bitcast_fusion.1
  33.0 9.7 %all_gather.12 = bf16[512,2,256]{2,0,1:T(8,128)(2,1)S(1)} all-gather(bf16[128,2,256]{2,0,1:T(8,128)(2,1)S(1)} %copy.62), channel_id=1, replica_groups=mesh['sp'=4,'tp'=8] {'sp'}, dimensions={0}, use_global_device_ids=true | all-gather | bytes 655360 | tf_op jit(solution)/shard_map/all_gather | solution.py:89
  44.4 9.7 %all_gather.13 = bf16[512,2,256]{2,0,1:T(8,128)(2,1)S(1)} all-gather(bf16[128,2,256]{2,0,1:T(8,128)(2,1)S(1)} %copy.63), channel_id=1, replica_groups=mesh['sp'=4,'tp'=8] {'sp'}, dimensions={0}, use_global_device_ids=true | all-gather | bytes 655360 | tf_op jit(solution)/shard_map/all_gather | solution.py:90
  56.1 1.8 fusion.2
  58.7 32.2 %reduce-scatter.3.cloned.1.call-done = bf16[16,4096]{1,0:T(8,128)(2,1)} async-done(((bf16[128,4096]{1,0:T(8,128)(2,1)}), bf16[16,4096]{1,0:T(8,128)(2,1)}) %reduce-scatter.3.cloned.1.call-update) | async-done | bytes 131088 | tf_op jit(solution)/shard_map/reduce_scatter | solution.py:101
  92.0 1.3 convolution_convert_fusion.1
  93.3 10.5 %all_to_all.10 = bf16[4,16,4096]{2,1,0:T(8,128)(2,1)S(1)} all-to-all(bf16[4,16,4096]{2,1,0:T(8,128)(2,1)S(1)} %bitcast.124), channel_id=1, replica_groups=mesh['sp'=4,'tp'=8] {'sp'}, dimensions={0} | all-to-all | bytes 1048576 | tf_op jit(solution)/shard_map/all_to_all | solution.py:135
  103.8 10.4 %collective-permute-done = bf16[4,16,4096]{2,1,0:T(8,128)(2,1)S(1)} collective-permute-done((bf16[4,16,4096]{2,1,0:T(8,128)(2,1)S(1)}, bf16[4,16,4096]{2,1,0:T(8,128)(2,1)S(1)}, u32[]{:S(2)}, u32[]{:S(2)}) %collective-permute-start) | collective-permute-done | bytes 524320 | tf_op jit(solution)/shard_map/ppermute | solution.py:138
  114.2 10.4 %collective-permute-done.1 = bf16[4,16,4096]{2,1,0:T(8,128)(2,1)S(1)} collective-permute-done((bf16[4,16,4096]{2,1,0:T(8,128)(2,1)S(1)}, bf16[4,16,4096]{2,1,0:T(8,128)(2,1)S(1)}, u32[]{:S(2)}, u32[]{:S(2)}) %collective-permute-start.1) | collective-permute-done | bytes 524320 | tf_op jit(solution)/shard_map/ppermute | solution.py:138
  125.4 10.4 %collective-permute-done.2 = bf16[4,16,4096]{2,1,0:T(8,128)(2,1)S(1)} collective-permute-done((bf16[4,16,4096]{2,1,0:T(8,128)(2,1)S(1)}, bf16[4,16,4096]{2,1,0:T(8,128)(2,1)S(1)}, u32[]{:S(2)}, u32[]{:S(2)}) %collective-permute-start.2) | collective-permute-done | bytes 524320 | tf_op jit(solution)/shard_map/ppermute | solution.py:138
  136.6 10.4 %collective-permute-done.3 = bf16[4,16,4096]{2,1,0:T(8,128)(2,1)S(1)} collective-permute-done((bf16[4,16,4096]{2,1,0:T(8,128)(2,1)S(1)}, bf16[4,16,4096]{2,1,0:T(8,128)(2,1)S(1)}, u32[]{:S(2)}, u32[]{:S(2)}) %collective-permute-start.3) | collective-permute-done | bytes 524320 | tf_op jit(solution)/shard_map/ppermute | solution.py:138
  147.8 10.4 %collective-permute-done.4 = bf16[4,16,4096]{2,1,0:T(8,128)(2,1)S(1)} collective-permute-done((bf16[4,16,4096]{2,1,0:T(8,128)(2,1)S(1)}, bf16[4,16,4096]{2,1,0:T(8,128)(2,1)S(1)}, u32[]{:S(2)}, u32[]{:S(2)}) %collective-permute-start.4) | collective-permute-done | bytes 524320 | tf_op jit(solution)/shard_map/ppermute | solution.py:138
  159.1 10.5 %collective-permute-done.5 = bf16[4,16,4096]{2,1,0:T(8,128)(2,1)} collective-permute-done((bf16[4,16,4096]{2,1,0:T(8,128)(2,1)S(1)}, bf16[4,16,4096]{2,1,0:T(8,128)(2,1)}, u32[]{:S(2)}, u32[]{:S(2)}) %collective-permute-start.5) | collective-permute-done | bytes 524320 | tf_op jit(solution)/shard_map/ppermute | solution.py:138
  169.6 10.7 %collective-permute-done.6 = bf16[4,16,4096]{2,1,0:T(8,128)(2,1)} collective-permute-done((bf16[4,16,4096]{2,1,0:T(8,128)(2,1)}, bf16[4,16,4096]{2,1,0:T(8,128)(2,1)}, u32[]{:S(2)}, u32[]{:S(2)}) %collective-permute-start.6) | collective-permute-done | bytes 524320 | tf_op jit(solution)/shard_map/ppermute | solution.py:138
  180.3 1.1 constant_dynamic-update-slice_fusion.15
  181.4 1.1 constant_dynamic-update-slice_fusion.14
  182.4 1.1 constant_dynamic-update-slice_fusion.13
  183.5 1.1 constant_dynamic-update-slice_fusion.12
  184.6 1.1 constant_dynamic-update-slice_fusion.11
  185.7 1.1 constant_dynamic-update-slice_fusion.10
  186.9 1.1 constant_dynamic-update-slice_fusion.7
  187.9 1.1 constant_dynamic-update-slice_fusion.6
  189.3 3.2 %copy-done.13 = bf16[64,16,4096]{2,1,0:T(8,128)(2,1)} copy-done((bf16[64,16,4096]{2,1,0:T(8,128)(2,1)}, bf16[64,16,4096]{2,1,0:T(8,128)(2,1)S(1)}, u32[]{:S(2)}) %copy-start.13) | copy-done | bytes 8388632
  192.6 1.3 fusion.15
  193.8 9.1 %fusion = bf16[32,2,8,4096]{3,2,0,1:T(8,128)(2,1)} fusion(bf16[2,256,4096]{2,1,0:T(8,128)(2,1)} %param.35, f32[32,2,8,256]{3,2,0,1:T(8,128)S(1)} %fusion.15, bf16[2,4096,256]{2,1,0:T(8,128)(2,1)} %param.34, bf16[64,16,4096]{2,1,0:T(8,128)(2,1)} %copy-done.13, s32[]{:T(128)S(6)} %select_n.37), kind=kOutput, calls=%fused_computation.2 | convolution fusion | flops 2150760448 | bytes 17301508 | tf_op jit(solution)/shard_map/necf,efd->necd/dot_general | solution.py:145
  202.9 4.6 %copy.121 = bf16[32,2,8,4096]{3,2,1,0:T(8,128)(2,1)} copy(bf16[32,2,8,4096]{3,2,0,1:T(8,128)(2,1)} %fusion) | data formatting | bytes 8388608 | tf_op jit(solution)/shard_map/convert_element_type | solution.py:146
  207.6 46.8 %reduce-scatter.5.cloned.1.call-done = bf16[4,16,4096]{2,1,0:T(8,128)(2,1)} async-done(((bf16[32,16,4096]{2,1,0:T(8,128)(2,1)}), bf16[4,16,4096]{2,1,0:T(8,128)(2,1)}) %reduce-scatter.5.cloned.1.call-update) | async-done | bytes 524304 | tf_op jit(solution)/shard_map/reduce_scatter | solution.py:147
  254.3 3.7 %all-to-all-start.1 = ((bf16[4,16,4096]{2,1,0:T(8,128)(2,1)}), bf16[4,16,4096]{2,1,0:T(8,128)(2,1)S(1)}, u32[]{:S(2)}, u32[]{:S(2)}) async-start(bf16[4,16,4096]{2,1,0:T(8,128)(2,1)} %reduce-scatter.5.cloned.1.call-done), calls=%async_computation.3 | async-start | bytes 1048576 | tf_op jit(solution)/shard_map/all_to_all | solution.py:153
  258.4 6.2 %all-to-all-done.1 = bf16[4,16,4096]{2,1,0:T(8,128)(2,1)S(1)} async-done(((bf16[4,16,4096]{2,1,0:T(8,128)(2,1)}), bf16[4,16,4096]{2,1,0:T(8,128)(2,1)S(1)}, u32[]{:S(2)}, u32[]{:S(2)}) %all-to-all-start.1) | async-done | bytes 524320 | tf_op jit(solution)/shard_map/all_to_all | solution.py:153
  (112 shorter events, 16.6 us)
Async XLA Ops:
  6.5 49.0 %copy-start = (bf16[256,4096]{1,0:T(8,128)(2,1)S(1)}, bf16[256,4096]{1,0:T(8,128)(2,1)}, u32[]{:S(2)}) copy-start(bf16[256,4096]{1,0:T(8,128)(2,1)} %param.28) | copy-start | bytes 6291460
  6.5 37.8 %copy-start.12 = (bf16[128,2,256]{2,1,0:T(2,128)(2,1)S(1)}, bf16[128,2,256]{2,1,0:T(2,128)(2,1)}, u32[]{:S(2)}) copy-start(bf16[128,2,256]{2,1,0:T(2,128)(2,1)} %param.20) | copy-start | bytes 393220
  6.5 49.0 %copy-start.18 = (f32[128]{0:T(128)S(1)}, f32[128]{0:T(128)}, u32[]{:S(2)}) copy-start(f32[128]{0:T(128)} %param.26) | copy-start | bytes 1540
  6.5 84.4 %reduce-scatter.3.cloned.1.call-start = ((), (), s32[]{:S(2)}) async-start(), calls=%async_computation.4 | async-start | bytes 1179648 | tf_op jit(solution)/shard_map/reduce_scatter | solution.py:101
  30.0 26.2 %copy-start.1 = (bf16[512,4096]{1,0:T(8,128)(2,1)S(1)}, bf16[512,4096]{1,0:T(8,128)(2,1)}, u32[]{:S(2)}) copy-start(bf16[512,4096]{1,0:T(8,128)(2,1)} %param.27) | copy-start | bytes 12582916
  30.0 26.2 %copy-start.16 = (f32[256]{0:T(256)S(1)}, f32[256]{0:T(256)}, u32[]{:S(2)}) copy-start(f32[256]{0:T(256)} %param.25) | copy-start | bytes 3076
  54.5 3.4 %copy-start.15 = (s32[16,2]{0,1:T(2,128)S(1)}, s32[16,2]{0,1:T(2,128)}, u32[]{:S(2)}) copy-start(s32[16,2]{0,1:T(2,128)} %param.31) | copy-start | bytes 388
  54.5 36.4 %copy-start.10 = (bf16[16,4096]{1,0:T(8,128)(2,1)S(1)}, bf16[16,4096]{1,0:T(8,128)(2,1)}, u32[]{:S(2)}) copy-start(bf16[16,4096]{1,0:T(8,128)(2,1)} %param.29) | copy-start | bytes 393220
  54.9 37.2 %copy-start.14 = (f32[4096]{0:T(1024)S(1)}, f32[4096]{0:T(1024)}, u32[]{:S(2)}) copy-start(f32[4096]{0:T(1024)} %param.30) | copy-start | bytes 49156
  57.9 196.4 %reduce-scatter.5.cloned.1.call-start = ((), (), s32[]{:S(2)}) async-start(), calls=%async_computation.5 | async-start | bytes 4718592 | tf_op jit(solution)/shard_map/reduce_scatter | solution.py:147
  103.8 10.4 %collective-permute-start = (bf16[4,16,4096]{2,1,0:T(8,128)(2,1)S(1)}, bf16[4,16,4096]{2,1,0:T(8,128)(2,1)S(1)}, u32[]{:S(2)}, u32[]{:S(2)}) collective-permute-start(bf16[4,16,4096]{2,1,0:T(8,128)(2,1)S(1)} %all_to_all.10), channel_id=1, source_target_pairs={{0,1},{1,2},{2,3},{3,4},{4,5},{5,6},{6,7},{7,0},{8,9},{9,10},{10,1... | collective-permute-start | bytes 1572872 | tf_op jit(solution)/shard_map/ppermute | solution.py:138
  114.2 10.4 %collective-permute-start.1 = (bf16[4,16,4096]{2,1,0:T(8,128)(2,1)S(1)}, bf16[4,16,4096]{2,1,0:T(8,128)(2,1)S(1)}, u32[]{:S(2)}, u32[]{:S(2)}) collective-permute-start(bf16[4,16,4096]{2,1,0:T(8,128)(2,1)S(1)} %collective-permute-done), channel_id=1, source_target_pairs={{0,1},{1,2},{2,3},{3,4},{4,5},{5,6},{6,7},{7,0},{8,9},{9,10},{10,1... | collective-permute-start | bytes 1572872 | tf_op jit(solution)/shard_map/ppermute | solution.py:138
  124.6 0.8 copy-start.2
  125.4 10.4 %collective-permute-start.2 = (bf16[4,16,4096]{2,1,0:T(8,128)(2,1)S(1)}, bf16[4,16,4096]{2,1,0:T(8,128)(2,1)S(1)}, u32[]{:S(2)}, u32[]{:S(2)}) collective-permute-start(bf16[4,16,4096]{2,1,0:T(8,128)(2,1)S(1)} %collective-permute-done.1), channel_id=1, source_target_pairs={{0,1},{1,2},{2,3},{3,4},{4,5},{5,6},{6,7},{7,0},{8,9},{9,10},{10,1... | collective-permute-start | bytes 1572872 | tf_op jit(solution)/shard_map/ppermute | solution.py:138
  135.8 0.8 copy-start.4
  136.6 10.4 %collective-permute-start.3 = (bf16[4,16,4096]{2,1,0:T(8,128)(2,1)S(1)}, bf16[4,16,4096]{2,1,0:T(8,128)(2,1)S(1)}, u32[]{:S(2)}, u32[]{:S(2)}) collective-permute-start(bf16[4,16,4096]{2,1,0:T(8,128)(2,1)S(1)} %collective-permute-done.2), channel_id=1, source_target_pairs={{0,1},{1,2},{2,3},{3,4},{4,5},{5,6},{6,7},{7,0},{8,9},{9,10},{10,1... | collective-permute-start | bytes 1572872 | tf_op jit(solution)/shard_map/ppermute | solution.py:138
  147.0 0.8 copy-start.6
  147.8 10.4 %collective-permute-start.4 = (bf16[4,16,4096]{2,1,0:T(8,128)(2,1)S(1)}, bf16[4,16,4096]{2,1,0:T(8,128)(2,1)S(1)}, u32[]{:S(2)}, u32[]{:S(2)}) collective-permute-start(bf16[4,16,4096]{2,1,0:T(8,128)(2,1)S(1)} %collective-permute-done.3), channel_id=1, source_target_pairs={{0,1},{1,2},{2,3},{3,4},{4,5},{5,6},{6,7},{7,0},{8,9},{9,10},{10,1... | collective-permute-start | bytes 1572872 | tf_op jit(solution)/shard_map/ppermute | solution.py:138
  158.2 0.8 copy-start.8
  159.1 10.5 %collective-permute-start.5 = (bf16[4,16,4096]{2,1,0:T(8,128)(2,1)S(1)}, bf16[4,16,4096]{2,1,0:T(8,128)(2,1)}, u32[]{:S(2)}, u32[]{:S(2)}) collective-permute-start(bf16[4,16,4096]{2,1,0:T(8,128)(2,1)S(1)} %collective-permute-done.4), channel_id=1, source_target_pairs={{0,1},{1,2},{2,3},{3,4},{4,5},{5,6},{6,7},{7,0},{8,9},{9,10},{10,1... | collective-permute-start | bytes 1572872 | tf_op jit(solution)/shard_map/ppermute | solution.py:138
  169.6 10.7 %collective-permute-start.6 = (bf16[4,16,4096]{2,1,0:T(8,128)(2,1)}, bf16[4,16,4096]{2,1,0:T(8,128)(2,1)}, u32[]{:S(2)}, u32[]{:S(2)}) collective-permute-start(bf16[4,16,4096]{2,1,0:T(8,128)(2,1)} %collective-permute-done.5), channel_id=1, source_target_pairs={{0,1},{1,2},{2,3},{3,4},{4,5},{5,6},{6,7},{7,0},{8,9},{9,10},{10,1... | collective-permute-start | bytes 1572872 | tf_op jit(solution)/shard_map/ppermute | solution.py:138
  169.6 19.5 %copy-start.9 = (bf16[4,16,4096]{2,1,0:T(8,128)(2,1)S(1)}, bf16[4,16,4096]{2,1,0:T(8,128)(2,1)}, u32[]{:S(2)}) copy-start(bf16[4,16,4096]{2,1,0:T(8,128)(2,1)} %copy-done.8) | copy-start | bytes 1572868
  169.6 19.5 %copy-start.7 = (bf16[4,16,4096]{2,1,0:T(8,128)(2,1)S(1)}, bf16[4,16,4096]{2,1,0:T(8,128)(2,1)}, u32[]{:S(2)}) copy-start(bf16[4,16,4096]{2,1,0:T(8,128)(2,1)} %copy-done.6) | copy-start | bytes 1572868
  169.6 19.6 %copy-start.5 = (bf16[4,16,4096]{2,1,0:T(8,128)(2,1)S(1)}, bf16[4,16,4096]{2,1,0:T(8,128)(2,1)}, u32[]{:S(2)}) copy-start(bf16[4,16,4096]{2,1,0:T(8,128)(2,1)} %copy-done.4) | copy-start | bytes 1572868
  169.6 19.6 %copy-start.3 = (bf16[4,16,4096]{2,1,0:T(8,128)(2,1)S(1)}, bf16[4,16,4096]{2,1,0:T(8,128)(2,1)}, u32[]{:S(2)}) copy-start(bf16[4,16,4096]{2,1,0:T(8,128)(2,1)} %copy-done.2) | copy-start | bytes 1572868
  169.6 23.0 %copy-start.19 = (bf16[2,4096,256]{2,1,0:T(8,128)(2,1)S(1)}, bf16[2,4096,256]{2,1,0:T(8,128)(2,1)}, u32[]{:S(2)}) copy-start(bf16[2,4096,256]{2,1,0:T(8,128)(2,1)} %param.33) | copy-start | bytes 12582916
  189.3 3.2 %copy-start.13 = (bf16[64,16,4096]{2,1,0:T(8,128)(2,1)}, bf16[64,16,4096]{2,1,0:T(8,128)(2,1)S(1)}, u32[]{:S(2)}) copy-start(bf16[64,16,4096]{2,1,0:T(8,128)(2,1)S(1)} %constant_dynamic-update-slice_fusion) | copy-start | bytes 25165828
  202.9 55.4 %copy-start.17 = (f32[16,2]{0,1:T(2,128)S(1)}, f32[16,2]{0,1:T(2,128)}, u32[]{:S(2)}) copy-start(f32[16,2]{0,1:T(2,128)} %param.32) | copy-start | bytes 388
  202.9 63.4 %copy-start.11 = (bf16[16,4096]{1,0:T(8,128)(2,1)S(1)}, bf16[16,4096]{1,0:T(8,128)(2,1)}, u32[]{:S(2)}) copy-start(bf16[16,4096]{1,0:T(8,128)(2,1)} %reduce-scatter.3.cloned.1.call-done) | copy-start | bytes 393220
  254.3 10.2 %all-to-all-start.1 = ((bf16[4,16,4096]{2,1,0:T(8,128)(2,1)}), bf16[4,16,4096]{2,1,0:T(8,128)(2,1)S(1)}, u32[]{:S(2)}, u32[]{:S(2)}) async-start(bf16[4,16,4096]{2,1,0:T(8,128)(2,1)} %reduce-scatter.5.cloned.1.call-done), calls=%async_computation.3 | async-start | bytes 1048576 | tf_op jit(solution)/shard_map/all_to_all | solution.py:153
Sparse Core Ops, SparseCore 0:
  58.0 32.8 reduce-scatter.2
  207.7 46.5 reduce-scatter.4
